TPU v7x, 512 devices: a whole 4x4x16 slice. The times are simulated.
512 devices in a mesh: sp: 64 (over z, y), tp: 8 (over x, core).
Axes of the slice: x: 4, y: 4, z: 16, core: 2. Of those that a mesh axis runs over, the one named last changes fastest.
Arguments:
- queries: bfloat16 [24576, 2048], P('sp', 'tp'), may hold values from -6 to 6
- key_heads: bfloat16 [24576, 1024], P('sp', 'tp'), may hold values from -6 to 6
- value_heads: bfloat16 [24576, 1024], P('sp', 'tp'), may hold values from -6 to 6
- sink_logit: float32 [16], P('tp'), may hold values from 3 to 7
- doc_ids: int32 [24576], replicated, may hold values from 0 to 15, never falling along the last dimension, each value on 1 to 3072 neighbouring positions
- residual: bfloat16 [24576, 2048], P('sp'), may hold values from -6 to 6
- out_proj: bfloat16 [2048, 2048], P('tp'), may hold values from -0.125 to 0.125
- gain_mix: float32 [2048], replicated, may hold values from 0.1 to 1.9
- up_proj: bfloat16 [2048, 8192], P('sp', 'tp'), may hold values from -0.125 to 0.125
- down_proj: bfloat16 [8192, 2048], P('tp', 'sp'), may hold values from -0.0625 to 0.0625
- gain_ffn_in: float32 [2048], replicated, may hold values from 0.1 to 1.9
- gain_ffn_out: float32 [2048], replicated, may hold values from 0.1 to 1.9
Outputs:
- layer_out: bfloat16 [24576, 2048], P(('sp', 'tp'))
All inputs are finite; a program needn't handle non-finite values.
Results may differ from a plain program's by a relative error of at most 0.019.
Values may be sent and summed in bfloat16 or wider, within the bound.
No kernel may reach another device: no remote copies, remote signals or barrier semaphores. Data moves between devices by JAX's collectives and lax.ppermute only.
A program may use at most 64 MiB of HBM per device.

v0:
```python
import jax
import jax.numpy as jnp
from jax import lax
from jax.sharding import PartitionSpec as P

HD = 128
WINDOW = 128


def turned_gather(arrays, axis, dims):
    turned = [jnp.moveaxis(a, dim, 0) for a, dim in zip(arrays, dims)]
    both = jnp.concatenate([t.reshape(len(t), -1) for t in turned], axis=1)
    result, at, gathered = (lax.all_gather(both, axis, axis=0, tiled=True), 0, [])
    for t, dim in zip(turned, dims):
        section = result[:, at : at + t[0].size].reshape(-1, *t.shape[1:])
        gathered.append(jnp.moveaxis(section, 0, dim))
        at += t[0].size
    return tuple(gathered)


def padded(shard, sides, width):
    for axis, dim in sides:
        devices, length = (lax.axis_size(axis), shard.shape[dim])
        up = [(i, (i + 1) % devices) for i in range(devices - 1)]
        down = [(j, i) for i, j in up]
        last = lax.slice_in_dim(shard, length - width, length, axis=dim)
        first = lax.slice_in_dim(shard, 0, width, axis=dim)
        before = lax.ppermute(last, axis, up)
        after = lax.ppermute(first, axis, down)
        shard = jnp.concatenate([before, shard, after], axis=dim)
    return shard


def split_up(shard, dim, devices):
    before, after = (shard.shape[:dim], shard.shape[dim + 1 :])
    return jnp.moveaxis(shard.reshape(*before, devices, -1, *after), dim, 0)


def summed_on_arrival(shard, axis, dim):
    pieces = split_up(shard, dim, lax.axis_size(axis))
    arrived = lax.all_to_all(pieces, axis, split_axis=0, concat_axis=0, tiled=True)
    return arrived.astype(jnp.float32).sum(axis=0)


def joined_along(pieces, dim):
    pieces = jnp.moveaxis(pieces, 0, dim)
    lengths = pieces.shape
    return pieces.reshape(*lengths[:dim], lengths[dim] * lengths[dim + 1], *lengths[dim + 2 :])


def copy_for_each(shard, axis):
    devices = lax.axis_size(axis)
    return lax.all_to_all(
        jnp.broadcast_to(shard[None], (devices, *shard.shape)), axis, 0, 0, tiled=True
    )


def collect(shard, axis, dim):
    return joined_along(copy_for_each(shard, axis), dim)


def rotate(field, places):
    half_dim = HD // 2
    inv_freq = 10000.0 ** (-jnp.arange(0, HD, 2, dtype=jnp.float32) / HD)
    angles = places[:, None, None] * inv_freq[None, None, :]
    cosine = jnp.cos(angles)
    sine = jnp.sin(angles)
    lower = field[..., :half_dim].astype(jnp.float32)
    upper = field[..., half_dim:].astype(jnp.float32)
    return jnp.concatenate(
        [lower * cosine - upper * sine, upper * cosine + lower * sine], axis=-1
    ).astype(jnp.bfloat16)


def banded(field, blocks):
    framed = field.reshape((blocks + 2, WINDOW) + field.shape[1:])
    return jnp.concatenate([framed[:-2], framed[1:-1], framed[2:]], axis=1)


def rms_scale(field, gain_vec):
    return field * lax.rsqrt(jnp.mean(field * field, axis=-1, keepdims=True) + 1e-06) * gain_vec


def body(
    queries,
    key_heads,
    value_heads,
    sink_logit,
    doc_ids,
    residual,
    out_proj,
    gain_mix,
    up_proj,
    down_proj,
    gain_ffn_in,
    gain_ffn_out,
):
    tok_count = queries.shape[0]
    blocks = tok_count // WINDOW
    share_rows = tok_count // lax.axis_size("tp")
    q_local = queries.shape[1] // HD
    kv_local = key_heads.shape[1] // HD
    group_size = q_local // kv_local
    offset = lax.axis_index("sp") * tok_count
    up_whole, down_whole = turned_gather((up_proj, down_proj), "sp", (0, 1))
    places = (offset + jnp.arange(tok_count)).astype(jnp.float32)
    rotated_q = rotate(queries.reshape(tok_count, q_local, HD), places).reshape(
        blocks, WINDOW, kv_local, group_size, HD
    )
    rotated_k = rotate(key_heads.reshape(tok_count, kv_local, HD), places).reshape(
        tok_count, kv_local * HD
    )
    rimmed = padded(jnp.stack([rotated_k, value_heads]), (("sp", 1),), WINDOW)
    key_win = banded(rimmed[0].reshape(-1, kv_local, HD), blocks)
    val_win = banded(rimmed[1].reshape(-1, kv_local, HD), blocks)
    padded_docs = jnp.pad(doc_ids, (WINDOW, WINDOW), constant_values=-1)
    key_docs = banded(lax.dynamic_slice_in_dim(padded_docs, offset, tok_count + 2 * WINDOW), blocks)
    query_docs = lax.dynamic_slice_in_dim(doc_ids, offset, tok_count).reshape(blocks, WINDOW)
    q_index = jnp.arange(WINDOW)[:, None]
    k_index = jnp.arange(3 * WINDOW)[None, :]
    in_window = jnp.abs(k_index - WINDOW - q_index) <= WINDOW
    allowed = (in_window[None] & (query_docs[:, :, None] == key_docs[:, None, :]))[:, None, None]
    scores = jnp.einsum(
        "nqkgd,nskd->nkgqs", rotated_q, key_win, preferred_element_type=jnp.float32
    ) * HD ** (-0.5)
    masked = jnp.where(allowed, scores, -1e30)
    sink_col = sink_logit.reshape(kv_local, group_size)[None, :, :, None]
    top_score = jnp.maximum(jnp.max(masked, axis=-1), sink_col)
    exp_scores = jnp.where(allowed, jnp.exp(masked - top_score[..., None]), 0.0)
    denom_sum = jnp.sum(exp_scores, axis=-1) + jnp.exp(sink_col - top_score)
    probs = (exp_scores / denom_sum[..., None]).astype(jnp.bfloat16)
    attn = (
        jnp.einsum("nkgqs,nskd->nqkgd", probs, val_win, preferred_element_type=jnp.float32)
        .astype(jnp.bfloat16)
        .reshape(tok_count, q_local * HD)
    )
    mixed = summed_on_arrival(
        jnp.dot(attn, out_proj, preferred_element_type=jnp.float32).astype(jnp.bfloat16), "tp", 0
    )
    own_resid = lax.dynamic_slice_in_dim(residual, lax.axis_index("tp") * share_rows, share_rows, 0)
    after_mix = (own_resid.astype(jnp.float32) + rms_scale(mixed, gain_mix)).astype(jnp.bfloat16)
    own_normed = rms_scale(after_mix.astype(jnp.float32), gain_ffn_in).astype(jnp.bfloat16)
    normed = collect(own_normed, "tp", 0)
    up_acts = jnp.dot(normed, up_whole, preferred_element_type=jnp.float32)
    hidden = jnp.square(jax.nn.relu(up_acts)).astype(jnp.bfloat16)
    ffn_out = summed_on_arrival(
        jnp.dot(hidden, down_whole, preferred_element_type=jnp.float32).astype(jnp.bfloat16),
        "tp",
        0,
    )
    return (after_mix.astype(jnp.float32) + rms_scale(ffn_out, gain_ffn_out)).astype(jnp.bfloat16)


def solution(mesh):
    return jax.shard_map(
        body,
        mesh=mesh,
        in_specs=(
            P("sp", "tp"),
            P("sp", "tp"),
            P("sp", "tp"),
            P("tp"),
            P(),
            P("sp", None),
            P("tp", None),
            P(),
            P("sp", "tp"),
            P("tp", "sp"),
            P(),
            P(),
        ),
        out_specs=P(("sp", "tp"), None),
        check_vma=False,
    )
```

profile of v0, /device:TPU:1, one launch (start us, length us, event | category | flops | bytes accessed | tf_op | source)
XLA Modules:
  0.0 213.6 jit_solution(9553838884716437725)
XLA Ops:
  6.5 1.6 pad_maximum_fusion
  8.2 1.8 fusion.41
  10.1 0.9 pad_maximum_fusion.11
  11.0 4.0 %collective-permute-start = (bf16[2,128,128]{2,1,0:T(8,128)(2,1)S(1)}, bf16[2,128,128]{2,1,0:T(8,128)(2,1)S(1)}, u32[]{:S(2)}, u32[]{:S(2)}) collective-permute-start(bf16[2,128,128]{2,1,0:T(8,128)(2,1)S(1)} %get-tuple-element.15), channel_id=1, source_target_pairs={{0,8},{8,16},{16,24},{24,32},{32,40},{40,48},{48,56},{56,64},{64,7... | collective-permute-start | bytes 196616 | tf_op jit(solution)/shard_map/ppermute | solution.py:28
  15.0 1.3 collective-permute-start.1
  16.3 1.1 copy.26
  17.7 0.4 multiply_cosine_fusion.1
  18.2 0.2 compare_and_fusion
  19.1 1.0 collective-permute-done.1
  20.4 0.4 fusion.53
  20.9 0.3 fusion.14
  21.3 0.4 fusion.13
  21.9 1.8 convolution_convert_fusion
  23.7 8.7 %all-to-all-start = ((bf16[8,48,2048]{2,1,0:T(8,128)(2,1)}), bf16[8,48,2048]{2,1,0:T(8,128)(2,1)S(1)}, u32[]{:S(2)}, u32[]{:S(2)}) async-start(bf16[8,48,2048]{2,1,0:T(8,128)(2,1)} %bitcast.63), calls=%async_computation | async-start | bytes 3145728 | tf_op jit(solution)/shard_map/all_to_all | solution.py:41
  32.5 20.6 %all-to-all-done = bf16[8,48,2048]{2,1,0:T(8,128)(2,1)S(1)} async-done(((bf16[8,48,2048]{2,1,0:T(8,128)(2,1)}), bf16[8,48,2048]{2,1,0:T(8,128)(2,1)S(1)}, u32[]{:S(2)}, u32[]{:S(2)}) %all-to-all-start) | async-done | bytes 1572896 | tf_op jit(solution)/shard_map/all_to_all | solution.py:41
  53.1 0.2 convert_reduce_fusion.1
  53.5 1.2 fusion.18
  55.0 24.0 %all_to_all.15 = bf16[8,48,2048]{2,1,0:T(8,128)(2,1)S(1)} all-to-all(bf16[8,48,2048]{2,1,0:T(8,128)(2,1)S(1)} %broadcast_in_dim.23), channel_id=1, replica_groups=mesh['sp'=64,'tp'=8] {'tp'}, dimensions={0} | all-to-all | bytes 3145728 | tf_op jit(solution)/shard_map/all_to_all | solution.py:53
  79.0 84.9 %all-gather.2.cloned.1.call-done = bf16[2048,2048]{1,0:T(8,128)(2,1)} async-done(((bf16[32,2048]{1,0:T(8,128)(2,1)}), bf16[2048,2048]{1,0:T(8,128)(2,1)}) %all-gather.2.cloned.1.call-update) | async-done | bytes 8388624 | tf_op jit(solution)/shard_map/all_gather | solution.py:13
  163.9 8.1 %fusion.4 = bf16[384,2048]{1,0:T(8,128)(2,1)} fusion(bf16[2048,2048]{1,0:T(8,128)(2,1)} %all-gather.2.cloned.1.call-done, bf16[384,2048]{1,0:T(8,128)(2,1)S(1)} %bitcast.64), kind=kOutput, calls=%fused_computation.6 | convolution fusion | flops 3223191552 | bytes 11534336 | tf_op jit(solution)/shard_map/dot_general | solution.py:147
  172.0 33.2 %all_to_all.16 = bf16[8,48,2048]{2,1,0:T(8,128)(2,1)S(1)} all-to-all(bf16[8,48,2048]{2,1,0:T(8,128)(2,1)} %bitcast.65), channel_id=1, replica_groups=mesh['sp'=64,'tp'=8] {'tp'}, dimensions={0} | all-to-all | bytes 3145728 | tf_op jit(solution)/shard_map/all_to_all | solution.py:41
  205.2 0.2 convert_reduce_fusion
  205.6 0.3 copy-done.4
  205.9 0.8 fusion.21
  (43 shorter events, 2.3 us)
Async XLA Ops:
  6.5 15.4 %copy-start = (bf16[256,2048]{1,0:T(8,128)(2,1)S(1)}, bf16[256,2048]{1,0:T(8,128)(2,1)}, u32[]{:S(2)}) copy-start(bf16[256,2048]{1,0:T(8,128)(2,1)} %param.18) | copy-start | bytes 3145732
  6.5 10.9 %copy-start.2 = (s32[24576]{0:T(1024)S(1)}, s32[24576]{0:T(1024)}, u32[]{:S(2)}) copy-start(s32[24576]{0:T(1024)} %param.16) | copy-start | bytes 294916
  6.5 157.3 %all-gather.2.cloned.1.call-start = ((), (), s32[]{:S(2)}) async-start(), calls=%async_computation.3 | async-start | bytes 8519680 | tf_op jit(solution)/shard_map/all_gather | solution.py:13
  10.1 8.9 %copy-start.1 = (bf16[384,128]{1,0:T(8,128)(2,1)S(1)}, bf16[384,128]{1,0:T(8,128)(2,1)}, u32[]{:S(2)}) copy-start(bf16[384,128]{1,0:T(8,128)(2,1)} %param.14) | copy-start | bytes 294916
  11.0 8.1 %collective-permute-start = (bf16[2,128,128]{2,1,0:T(8,128)(2,1)S(1)}, bf16[2,128,128]{2,1,0:T(8,128)(2,1)S(1)}, u32[]{:S(2)}, u32[]{:S(2)}) collective-permute-start(bf16[2,128,128]{2,1,0:T(8,128)(2,1)S(1)} %get-tuple-element.15), channel_id=1, source_target_pairs={{0,8},{8,16},{16,24},{24,32},{32,40},{40,48},{48,56},{56,64},{64,7... | collective-permute-start | bytes 196616 | tf_op jit(solution)/shard_map/ppermute | solution.py:28
  15.0 5.0 %collective-permute-start.1 = (bf16[2,128,128]{2,1,0:T(8,128)(2,1)S(1)}, bf16[2,128,128]{2,1,0:T(8,128)(2,1)S(1)}, u32[]{:S(2)}, u32[]{:S(2)}) collective-permute-start(bf16[2,128,128]{2,1,0:T(8,128)(2,1)S(1)} %get-tuple-element.16), channel_id=1, source_target_pairs={{8,0},{16,8},{24,16},{32,24},{40,32},{48,40},{56,48},{64,56},{72,6... | collective-permute-start | bytes 196616 | tf_op jit(solution)/shard_map/ppermute | solution.py:29
  20.1 0.7 copy-start.6
  23.7 29.4 %all-to-all-start = ((bf16[8,48,2048]{2,1,0:T(8,128)(2,1)}), bf16[8,48,2048]{2,1,0:T(8,128)(2,1)S(1)}, u32[]{:S(2)}, u32[]{:S(2)}) async-start(bf16[8,48,2048]{2,1,0:T(8,128)(2,1)} %bitcast.63), calls=%async_computation | async-start | bytes 3145728 | tf_op jit(solution)/shard_map/all_to_all | solution.py:41
  32.5 21.0 %copy-start.3 = (f32[2048]{0:T(1024)S(1)}, f32[2048]{0:T(1024)}, u32[]{:S(2)}) copy-start(f32[2048]{0:T(1024)} %param.19) | copy-start | bytes 24580
  32.5 22.2 %copy-start.5 = (f32[2048]{0:T(1024)S(1)}, f32[2048]{0:T(1024)}, u32[]{:S(2)}) copy-start(f32[2048]{0:T(1024)} %param.22) | copy-start | bytes 24580
  205.2 0.7 copy-start.4
Sparse Core Ops, SparseCore 0:
  10.3 153.5 all-gather.1
where the time goes:
time: 214 us
  waiting for transfers between devices  106 us (50%)
  blocking collectives  57.2 us (27%)
  starting transfers between devices  14.1 us (7%)
  between operations  13.6 us (6%)
  matrix products  10.8 us (5%)
  other arithmetic  8.61 us (4%)
  local copies, waits for them, and re-layouts  2.78 us (1%)
    all_gather x1, waiting for transfers between devices, turned_gather(): lax.all_gather(both, axis, axis=0, tiled=True)  84.9 us
    all_to_all x1, blocking collectives, summed_on_arrival(): lax.all_to_all(pieces, axis, split_axis=0, concat_axis=0, tiled=True)  33.2 us
    all_to_all x1, blocking collectives, copy_for_each(): lax.all_to_all(jnp.broadcast_to(shard[None], (devices, *shard.shape)), ax...  24 us
    all_to_all x1, waiting for transfers between devices, summed_on_arrival(): lax.all_to_all(pieces, axis, split_axis=0, concat_axis=0, tiled=True)  20.6 us
    all_to_all x1, starting transfers between devices, summed_on_arrival(): lax.all_to_all(pieces, axis, split_axis=0, concat_axis=0, tiled=True)  8.74 us
    dot_general x1, matrix products, body(): jnp.dot(hidden, down_whole, preferred_element_type=jnp.float32)  8.11 us
  transfers between devices with their start and end apart: 4, of which 3 were waited for; matrix products, arithmetic and copies ran while one was open for 5% of the time, Pallas kernels for 0%

commit v1 on v0

--- a/solution.py
+++ b/solution.py
@@ -10,7 +10,13 @@
 def turned_gather(arrays, axis, dims):
     turned = [jnp.moveaxis(a, dim, 0) for a, dim in zip(arrays, dims)]
     both = jnp.concatenate([t.reshape(len(t), -1) for t in turned], axis=1)
-    result, at, gathered = (lax.all_gather(both, axis, axis=0, tiled=True), 0, [])
+    result, at, gathered = (
+        jnp.concatenate(
+            lax.all_to_all(jnp.stack([both] * lax.axis_size(axis)), axis, 0, 0), axis=0
+        ),
+        0,
+        [],
+    )
     for t, dim in zip(turned, dims):
         section = result[:, at : at + t[0].size].reshape(-1, *t.shape[1:])
         gathered.append(jnp.moveaxis(section, 0, dim))

time: 214 us -> 497 us (2.32)
  blocking collectives: 57.2 us -> 413 us
  waiting for transfers between devices: 106 us -> 41.2 us
  between operations: 13.6 us -> 0.26 us
    all_to_all x1, blocking collectives: 24 us -> 382 us  [turned_gather(): lax.all_to_all(jnp.stack([both] * lax.axis_size(axis)), axis, 0, 0)]
    all_gather x1 -> x0, waiting for transfers between devices: 84.9 us -> none  [turned_gather(): lax.all_gather(both, axis, axis=0, tiled=True)]
    all_to_all x0 -> x1, waiting for transfers between devices: none -> 20.6 us  [copy_for_each(): lax.all_to_all(jnp.broadcast_to(shard[None], (devices, *shard.shape)), ax...]
  transfers between devices with their start and end apart: 4 -> 4, of which waited for: 3 -> 2; matrix products, arithmetic and copies ran while one was open for 5% -> 1% of each run, Pallas kernels for 0% -> 0%
where the time goes in v1:
time: 497 us
  blocking collectives  413 us (83%)
  waiting for transfers between devices  41.2 us (8%)
  starting transfers between devices  18.2 us (4%)
  matrix products  10.7 us (2%)
  other arithmetic  7.02 us (1%)
  local copies, waits for them, and re-layouts  6.6 us (1%)
    all_to_all x1, blocking collectives, turned_gather(): lax.all_to_all(jnp.stack([both] * lax.axis_size(axis)), axis, 0, 0)  382 us
    all_to_all x1, blocking collectives, summed_on_arrival(): lax.all_to_all(pieces, axis, split_axis=0, concat_axis=0, tiled=True)  30.5 us
    all_to_all x1, waiting for transfers between devices, summed_on_arrival(): lax.all_to_all(pieces, axis, split_axis=0, concat_axis=0, tiled=True)  20.6 us
    all_to_all x1, waiting for transfers between devices, copy_for_each(): lax.all_to_all(jnp.broadcast_to(shard[None], (devices, *shard.shape)), ax...  20.6 us
  transfers between devices with their start and end apart: 4, of which 2 were waited for; matrix products, arithmetic and copies ran while one was open for 1% of the time, Pallas kernels for 0%

profile of v1, /device:TPU:1, one launch (start us, length us, event | category | flops | bytes accessed | tf_op | source)
XLA Modules:
  0.0 496.6 jit_solution(8760267173744208834)
XLA Ops:
  0.0 1.9 fusion.41
  1.9 0.9 pad_maximum_fusion.11
  2.8 4.0 collective-permute-start
  6.9 1.3 collective-permute-start.1
  8.2 0.4 multiply_cosine_fusion.1
  8.6 1.1 copy.26
  9.7 0.8 pad_dynamic-slice_fusion
  10.5 0.8 dynamic-slice_bitcast_fusion
  12.5 0.4 fusion.53
  13.2 0.3 fusion.14
  13.8 0.4 fusion.13
  14.4 1.7 convolution_convert_fusion
  16.1 8.3 %all-to-all-start = ((bf16[8,48,2048]{2,1,0:T(8,128)(2,1)}), bf16[8,48,2048]{2,1,0:T(8,128)(2,1)S(1)}, u32[]{:S(2)}, u32[]{:S(2)}) async-start(bf16[8,48,2048]{2,1,0:T(8,128)(2,1)} %bitcast.65), calls=%async_computation | async-start | bytes 3145728 | tf_op jit(solution)/shard_map/all_to_all | solution.py:47
  24.4 20.6 %all-to-all-done = bf16[8,48,2048]{2,1,0:T(8,128)(2,1)S(1)} async-done(((bf16[8,48,2048]{2,1,0:T(8,128)(2,1)}), bf16[8,48,2048]{2,1,0:T(8,128)(2,1)S(1)}, u32[]{:S(2)}, u32[]{:S(2)}) %all-to-all-start) | async-done | bytes 1572896 | tf_op jit(solution)/shard_map/all_to_all | solution.py:47
  45.4 1.2 fusion.18
  46.8 1.3 broadcast_in_dim.23
  48.1 4.6 all-to-all-start.1
  52.7 20.6 %all-to-all-done.1 = bf16[8,48,2048]{2,1,0:T(8,128)(2,1)S(1)} async-done(((bf16[8,48,2048]{2,1,0:T(8,128)(2,1)}), bf16[8,48,2048]{2,1,0:T(8,128)(2,1)S(1)}, u32[]{:S(2)}, u32[]{:S(2)}) %all-to-all-start.1) | async-done | bytes 1572896 | tf_op jit(solution)/shard_map/all_to_all | solution.py:59
  73.3 1.1 stack.8
  74.4 382.1 %all_to_all.20 = bf16[64,32,2048]{2,1,0:T(8,128)(2,1)} all-to-all(bf16[64,32,2048]{2,1,0:T(8,128)(2,1)S(1)} %stack.8), channel_id=1, replica_groups=mesh['sp'=64,'tp'=8] {'sp'}, dimensions={0} | all-to-all | bytes 16777216 | tf_op jit(solution)/shard_map/all_to_all | solution.py:15
  456.5 8.1 %fusion.4 = bf16[384,2048]{1,0:T(8,128)(2,1)} fusion(bf16[2048,2048]{1,0:T(8,128)(2,1)} %bitcast.64, bf16[384,2048]{1,0:T(8,128)(2,1)S(1)} %bitcast.66), kind=kOutput, calls=%fused_computation.6 | convolution fusion | flops 3223191552 | bytes 11534336 | tf_op jit(solution)/shard_map/dot_general | solution.py:153
  464.6 30.5 %all_to_all.21 = bf16[8,48,2048]{2,1,0:T(8,128)(2,1)S(1)} all-to-all(bf16[8,48,2048]{2,1,0:T(8,128)(2,1)} %bitcast.67), channel_id=1, replica_groups=mesh['sp'=64,'tp'=8] {'tp'}, dimensions={0} | all-to-all | bytes 3145728 | tf_op jit(solution)/shard_map/all_to_all | solution.py:47
  495.5 0.3 copy-done.5
  495.8 0.8 fusion.21
  (45 shorter events, 2.8 us)
Async XLA Ops:
  0.0 14.4 %copy-start = (bf16[256,2048]{1,0:T(8,128)(2,1)S(1)}, bf16[256,2048]{1,0:T(8,128)(2,1)}, u32[]{:S(2)}) copy-start(bf16[256,2048]{1,0:T(8,128)(2,1)} %param.18) | copy-start | bytes 3145732
  1.9 10.3 %copy-start.1 = (bf16[384,128]{1,0:T(8,128)(2,1)S(1)}, bf16[384,128]{1,0:T(8,128)(2,1)}, u32[]{:S(2)}) copy-start(bf16[384,128]{1,0:T(8,128)(2,1)} %param.14) | copy-start | bytes 294916
  2.8 9.5 %collective-permute-start = (bf16[2,128,128]{2,1,0:T(8,128)(2,1)S(1)}, bf16[2,128,128]{2,1,0:T(8,128)(2,1)S(1)}, u32[]{:S(2)}, u32[]{:S(2)}) collective-permute-start(bf16[2,128,128]{2,1,0:T(8,128)(2,1)S(1)} %get-tuple-element.15), channel_id=1, source_target_pairs={{0,8},{8,16},{16,24},{24,32},{32,40},{40,48},{48,56},{56,64},{64,7... | collective-permute-start | bytes 196616 | tf_op jit(solution)/shard_map/ppermute | solution.py:34
  6.9 5.4 %collective-permute-start.1 = (bf16[2,128,128]{2,1,0:T(8,128)(2,1)S(1)}, bf16[2,128,128]{2,1,0:T(8,128)(2,1)S(1)}, u32[]{:S(2)}, u32[]{:S(2)}) collective-permute-start(bf16[2,128,128]{2,1,0:T(8,128)(2,1)S(1)} %get-tuple-element.16), channel_id=1, source_target_pairs={{8,0},{16,8},{24,16},{32,24},{40,32},{48,40},{56,48},{64,56},{72,6... | collective-permute-start | bytes 196616 | tf_op jit(solution)/shard_map/ppermute | solution.py:35
  12.4 0.7 copy-start.7
  16.1 28.9 %all-to-all-start = ((bf16[8,48,2048]{2,1,0:T(8,128)(2,1)}), bf16[8,48,2048]{2,1,0:T(8,128)(2,1)S(1)}, u32[]{:S(2)}, u32[]{:S(2)}) async-start(bf16[8,48,2048]{2,1,0:T(8,128)(2,1)} %bitcast.65), calls=%async_computation | async-start | bytes 3145728 | tf_op jit(solution)/shard_map/all_to_all | solution.py:47
  24.4 21.0 %copy-start.4 = (f32[2048]{0:T(1024)S(1)}, f32[2048]{0:T(1024)}, u32[]{:S(2)}) copy-start(f32[2048]{0:T(1024)} %param.19) | copy-start | bytes 24580
  24.4 22.2 %copy-start.6 = (f32[2048]{0:T(1024)S(1)}, f32[2048]{0:T(1024)}, u32[]{:S(2)}) copy-start(f32[2048]{0:T(1024)} %param.22) | copy-start | bytes 24580
  48.1 4.6 copy-start.2
  48.1 4.6 copy-start.3
  48.1 25.2 %all-to-all-start.1 = ((bf16[8,48,2048]{2,1,0:T(8,128)(2,1)}), bf16[8,48,2048]{2,1,0:T(8,128)(2,1)S(1)}, u32[]{:S(2)}, u32[]{:S(2)}) async-start(bf16[8,48,2048]{2,1,0:T(8,128)(2,1)} %broadcast_in_dim.23), calls=%async_computation.1 | async-start | bytes 3145728 | tf_op jit(solution)/shard_map/all_to_all | solution.py:59
  495.1 0.7 copy-start.5
